TPU v7x, 32 devices: a whole 2x2x4 slice. The times are simulated.
32 devices in a mesh: kv: 8 (over z, y), tp: 4 (over x, core).
Axes of the slice: x: 2, y: 2, z: 4, core: 2. Of those that a mesh axis runs over, the one named last changes fastest.
Arguments:
- tokens: bfloat16 [128, 4096], P('kv'), may hold values from -6 to 6
- dec_tokens: bfloat16 [8, 4096], P('kv'), may hold values from -6 to 6
- norm_gain: float32 [4096], replicated, may hold values from 0.1 to 1.9
- w_query: bfloat16 [2, 4096, 1024], P(None, None, 'tp'), may hold values from -0.09375 to 0.09375
- w_key: bfloat16 [2, 4096, 1024], P(None, None, 'tp'), may hold values from -0.15625 to 0.15625
- w_value: bfloat16 [4096, 2048], P(None, 'tp'), may hold values from -0.09375 to 0.09375
- w_out: bfloat16 [2048, 4096], P('tp'), may hold values from -0.125 to 0.125
- head_gain: float32 [256], replicated, may hold values from 0.1 to 1.9
- mix_lambda: float32 [8], P('tp'), may hold values from 0.3 to 0.8
- ctx_keys: bfloat16 [2, 8192, 1024], P(None, 'kv', 'tp'), may hold values from -600 to 600
- ctx_values: bfloat16 [8192, 2048], P('kv', 'tp'), may hold values from -6 to 6
- dec_keys: bfloat16 [2, 8, 2048, 1024], P(None, 'kv', None, 'tp'), may hold values from -600 to 600
- dec_values: bfloat16 [8, 2048, 2048], P('kv', None, 'tp'), may hold values from -6 to 6
- dec_len: int32 [8], P('kv'), may hold values from 256 to 2048, as said below
Outputs:
- piece_out: bfloat16 [128, 4096], P('kv', 'tp')
- dec_out: bfloat16 [8, 4096], P('kv', 'tp')
Inputs may be any that keep to these rules, and one draw needn't show every extreme that they name: `dec_len`: some decoding sequence has exactly 2048 cached positions.
All inputs are finite; a program needn't handle non-finite values.
Results may differ from a plain program's by a relative error of at most 0.03.
The roundings to bfloat16 on the way count: a program that leaves them out, or rounds other values in their place, can miss the bound.
Values may be sent and summed in bfloat16 or wider, within the bound.
No kernel may reach another device: no remote copies, remote signals or barrier semaphores. Data moves between devices by JAX's collectives and lax.ppermute only.
A program may use at most 64 MiB of HBM per device.

v0:
```python
import math

import jax
import jax.numpy as jnp
from jax import lax
from jax.sharding import PartitionSpec as P

DH = 128


epsilon = 1e-06


def map_scores(block, ctx_keys, own_keys, block_pos, own_pos, cols, scale):
    pairs = []
    for part in range(2):
        query = block[:, part, cols]
        far = (
            jnp.einsum(
                "nd,md->nm", query, ctx_keys[part][:, cols], preferred_element_type=jnp.float32
            )
            * scale
        )
        near = (
            jnp.einsum(
                "nd,md->nm", query, own_keys[:, part, cols], preferred_element_type=jnp.float32
            )
            * scale
        )
        near = jnp.where(own_pos[None, :] <= block_pos[:, None], near, -jnp.inf)
        pairs.append((far, near))
    return pairs


def body(
    tokens,
    dec_tokens,
    norm_gain,
    w_query,
    w_key,
    w_value,
    w_out,
    head_gain,
    mix_lambda,
    ctx_keys,
    ctx_values,
    dec_keys,
    dec_values,
    dec_len,
):
    scale = DH ** (-0.5)
    local_heads = mix_lambda.shape[0]
    piece_rows = tokens.shape[0]
    dec_rows = dec_tokens.shape[0]
    rows = jnp.concatenate([tokens, dec_tokens], axis=0)
    xf = rows.astype(jnp.float32)
    normed = (
        xf * lax.rsqrt(jnp.mean(xf * xf, axis=-1, keepdims=True) + epsilon) * norm_gain
    ).astype(jnp.bfloat16)
    query = jnp.einsum("rd,cdn->rcn", normed, w_query, preferred_element_type=jnp.float32).astype(
        jnp.bfloat16
    )
    keys = jnp.einsum("rd,cdn->rcn", normed, w_key, preferred_element_type=jnp.float32).astype(
        jnp.bfloat16
    )
    value = jnp.dot(normed, w_value, preferred_element_type=jnp.float32).astype(jnp.bfloat16)
    own_keys = keys[:piece_rows]
    own_values = value[:piece_rows]
    own_pos = lax.axis_index("kv") * piece_rows + jnp.arange(piece_rows, dtype=jnp.int32)
    gathered = lax.all_gather(query[:piece_rows], "kv", axis=0, tiled=True)
    total_rows = gathered.shape[0]
    width = gathered.shape[2]
    block = math.gcd(total_rows, 512)
    blocks = total_rows // block
    query_blocks = gathered.reshape(blocks, block, 2, width)
    pos_blocks = jnp.arange(total_rows, dtype=jnp.int32).reshape(blocks, block)

    def block_stats(args):
        qb, qpos = args
        maxima, totals = ([], [])
        for head in range(local_heads):
            cols = slice(head * DH, (head + 1) * DH)
            for far, near in map_scores(qb, ctx_keys, own_keys, qpos, own_pos, cols, scale):
                top = jnp.maximum(jnp.max(far, axis=-1), jnp.max(near, axis=-1))
                maxima.append(top)
                totals.append(
                    jnp.sum(jnp.exp(far - top[:, None]), axis=-1)
                    + jnp.sum(jnp.exp(near - top[:, None]), axis=-1)
                )
        return (jnp.stack(maxima), jnp.stack(totals))

    local_max, local_tot = lax.map(block_stats, (query_blocks, pos_blocks))
    local_max = jnp.moveaxis(local_max, 0, 1).reshape(2 * local_heads, total_rows)
    local_tot = jnp.moveaxis(local_tot, 0, 1).reshape(2 * local_heads, total_rows)
    row_top = lax.pmax(local_max, "kv")
    row_sum = lax.psum(local_tot * jnp.exp(local_max - row_top), "kv")

    def block_terms(qb, qpos, top_b, sum_b):
        outputs = []
        for head in range(local_heads):
            cols = slice(head * DH, (head + 1) * DH)
            vcols = slice(head * 2 * DH, (head + 1) * 2 * DH)
            pairs = map_scores(qb, ctx_keys, own_keys, qpos, own_pos, cols, scale)
            shares = []
            for part in range(2):
                far, near = pairs[part]
                top = top_b[2 * head + part][:, None]
                denom = sum_b[2 * head + part][:, None]
                shares.append((jnp.exp(far - top) / denom, jnp.exp(near - top) / denom))
            lam = mix_lambda[head]
            far_w = (shares[0][0] - lam * shares[1][0]).astype(jnp.bfloat16)
            near_w = (shares[0][1] - lam * shares[1][1]).astype(jnp.bfloat16)
            outputs.append(
                jnp.dot(far_w, ctx_values[:, vcols], preferred_element_type=jnp.float32)
                + jnp.dot(near_w, own_values[:, vcols], preferred_element_type=jnp.float32)
            )
        return jnp.concatenate(outputs, axis=-1)

    top_blocks = jnp.moveaxis(row_top.reshape(2 * local_heads, blocks, block), 1, 0)
    sum_blocks = jnp.moveaxis(row_sum.reshape(2 * local_heads, blocks, block), 1, 0)
    terms = lax.map(
        lambda args: block_terms(*args), (query_blocks, pos_blocks, top_blocks, sum_blocks)
    )
    piece_att = lax.psum_scatter(
        terms.reshape(total_rows, terms.shape[2]), "kv", scatter_dimension=0, tiled=True
    )
    dec_query = query[piece_rows:].reshape(dec_rows, 2, local_heads, DH)
    dec_new_k = keys[piece_rows:].reshape(dec_rows, 2, local_heads, DH)
    dec_new_v = value[piece_rows:].reshape(dec_rows, local_heads, 2 * DH)
    slots = dec_keys.shape[2]
    cache_k = dec_keys.reshape(2, dec_rows, slots, local_heads, DH)
    far = (
        jnp.einsum("bchd,cbjhd->bchj", dec_query, cache_k, preferred_element_type=jnp.float32)
        * scale
    )
    valid = jnp.arange(slots, dtype=jnp.int32)[None, :] < dec_len[:, None]
    far = jnp.where(valid[:, None, None, :], far, -jnp.inf)
    near = (
        jnp.einsum("bchd,bchd->bch", dec_query, dec_new_k, preferred_element_type=jnp.float32)
        * scale
    )
    top = jnp.maximum(jnp.max(far, axis=-1), near)
    denom = jnp.sum(jnp.exp(far - top[..., None]), axis=-1) + jnp.exp(near - top)
    far_p = jnp.exp(far - top[..., None]) / denom[..., None]
    near_p = jnp.exp(near - top) / denom
    far_w = (far_p[:, 0] - mix_lambda[None, :, None] * far_p[:, 1]).astype(jnp.bfloat16)
    near_w = (near_p[:, 0] - mix_lambda[None, :] * near_p[:, 1]).astype(jnp.bfloat16)
    cache_v = dec_values.reshape(dec_rows, slots, local_heads, 2 * DH)
    dec_att = jnp.einsum("bhj,bjhe->bhe", far_w, cache_v, preferred_element_type=jnp.float32)
    dec_att = dec_att + near_w.astype(jnp.float32)[..., None] * dec_new_v.astype(jnp.float32)
    attended = jnp.concatenate(
        [piece_att.reshape(piece_rows, local_heads, 2 * DH), dec_att], axis=0
    )
    heads_out = (
        attended
        * lax.rsqrt(jnp.mean(attended * attended, axis=-1, keepdims=True) + epsilon)
        * head_gain
    )
    heads_out = heads_out.astype(jnp.bfloat16).reshape(piece_rows + dec_rows, local_heads * 2 * DH)
    partial_value = jnp.dot(heads_out, w_out, preferred_element_type=jnp.float32)
    partial_value = lax.optimization_barrier(partial_value.astype(jnp.bfloat16)).astype(jnp.float32)
    summed = lax.psum_scatter(
        partial_value.astype(jnp.bfloat16), "tp", scatter_dimension=1, tiled=True
    )
    return (summed[:piece_rows], summed[piece_rows:])


def solution(mesh):
    in_specs = (
        P("kv", None),
        P("kv", None),
        P(),
        P(None, None, "tp"),
        P(None, None, "tp"),
        P(None, "tp"),
        P("tp", None),
        P(),
        P("tp"),
        P(None, "kv", "tp"),
        P("kv", "tp"),
        P(None, "kv", None, "tp"),
        P("kv", None, "tp"),
        P("kv"),
    )
    out_specs = (P("kv", "tp"), P("kv", "tp"))
    return jax.shard_map(body, mesh=mesh, in_specs=in_specs, out_specs=out_specs, check_vma=False)
```

profile of v0, /device:TPU:0, one launch (start us, length us, event | category | flops | bytes accessed | tf_op | source)
XLA Modules:
  0.0 190.0 jit_solution(14455661820327340171)
XLA Ops:
  7.2 0.0 copy-start
  7.2 0.0 copy-start.2
  7.2 0.0 copy-start.4
  7.2 0.0 copy-start.5
  7.2 0.0 reduce-scatter.3.cloned.1.call-start
  7.3 0.0 copy-start.1
  7.3 1.2 fusion.8
  8.5 0.0 copy-start.3
  8.5 3.1 %convolution_convert_fusion.3 = bf16[17,2,256]{2,0,1:T(8,128)(2,1)S(1)} fusion(bf16[2,4096,256]{2,1,0:T(8,128)(2,1)} %param.17, f32[4096]{0:T(1024)} %param.16, f32[17]{0:T(128)S(1)} %add_rsqrt_fusion.1, bf16[1,4096]{1,0:T(2,128)(2,1)} %param.15, bf16[16,4096]{1,0:T(8,128)(2,1)} %param.14), kind=kOutput, calls=%fused_computation.11 | convolution fusion | flops 71799296 | bytes 4367428 | tf_op jit(solution)/shard_map/rd,cdn->rcn/dot_general | solution.py:60
  11.6 32.3 %all_gather.3 = bf16[128,2,256]{2,0,1:T(8,128)(2,1)S(1)} all-gather(bf16[16,2,256]{2,0,1:T(8,128)(2,1)S(1)} %slice.222), channel_id=1, replica_groups=mesh['kv'=8,'tp'=4] {'kv'}, dimensions={0}, use_global_device_ids=true | all-gather | bytes 147456 | tf_op jit(solution)/shard_map/all_gather | solution.py:70
  44.0 0.0 copy-done.2
  44.0 0.0 copy-done.4
  44.0 0.0 copy-done.5
  44.0 0.0 copy-done.1
  44.0 0.7 convolution_convert_fusion.2
  44.7 0.1 fusion.63
  44.9 0.2 fusion.65
  45.0 0.2 fusion.59
  45.2 0.0 copy-done.3
  45.2 0.1 slice_bitcast_fusion.1
  45.3 0.3 fusion.62
  45.6 0.3 fusion.58
  45.9 0.0 copy-start.6
  46.0 0.1 fusion.61
  46.1 0.3 fusion.64
  46.4 0.3 fusion.60
  46.8 0.2 exponential_reduce_fusion.2
  47.1 0.2 exponential_reduce_fusion.3
  47.3 0.2 exponential_reduce_fusion
  47.6 0.2 exponential_reduce_fusion.1
  47.9 21.4 %pmax.7 = f32[4,128]{1,0:T(4,128)S(1)} all-reduce(f32[4,128]{1,0:T(4,128)S(1)} %pad_maximum_fusion.2), channel_id=1, replica_groups=mesh['kv'=8,'tp'=4] {'kv'}, use_global_device_ids=true, to_apply=%region_9.10 | all-reduce | flops 512 | bytes 4096 | tf_op jit(solution)/shard_map/pmax | solution.py:95
  69.3 17.1 %psum.7 = f32[4,128]{1,0:T(4,128)S(1)} all-reduce(f32[4,128]{1,0:T(4,128)S(1)} %maximum_multiply_fusion.2), channel_id=1, replica_groups=mesh['kv'=8,'tp'=4] {'kv'}, use_global_device_ids=true, to_apply=%region_18.19 | all-reduce | flops 512 | bytes 4096 | tf_op jit(solution)/shard_map/psum | solution.py:96
  86.4 0.0 copy-start.7
  86.4 3.0 %convolution_convert_fusion.1 = bf16[17,512]{1,0:T(8,128)(2,1)S(1)} fusion(bf16[4096,512]{1,0:T(8,128)(2,1)} %param.19, f32[4096]{0:T(1024)S(1)} %copy-done.5, f32[17]{0:T(128)S(1)} %add_rsqrt_fusion.1, bf16[1,4096]{1,0:T(2,128)(2,1)S(1)} %copy-done.4, bf16[16,4096]{1,0:T(8,128)(2,1)S(1)} %copy-done.2), kind=kOutput, calls=%fused_computation.9 | convolution fusion | flops 71799296 | bytes 4367428 | tf_op jit(solution)/shard_map/dot_general | solution.py:66
  89.4 0.0 copy-done.6
  89.4 0.6 fusion.57
  90.0 0.8 fusion.30
  90.8 2.1 %convolution_add_fusion.1 = f32[128,256]{1,0:T(8,128)S(1)} fusion(f32[128,256]{1,0:T(8,128)S(1)} %fusion.30, bf16[1024,512]{1,0:T(8,128)(2,1)} %param.24, f32[128,1024]{1,0:T(8,128)S(1)} %get-tuple-element.85, f32[128,1024]{1,0:T(8,128)S(1)} %get-tuple-element.89, f32[128]{0:T(128)S(1)} %get-tuple-element.61, f32[128]{0:T(128)S(1)} %get-tuple-element.57, ...), kind=kOutput, calls=%fused_computation.8 | convolution fusion | flops 68059136 | bytes 1837568 | tf_op jit(solution)/shard_map/while/body/eval_jaxpr/dot_general | solution.py:114
  92.9 0.9 fusion.28
  93.8 0.0 copy-done.7
  93.8 1.0 convolution_add_fusion
  94.8 0.7 pad_maximum_fusion
  95.6 0.0 reduce-scatter.3.cloned.1.call-update
  95.6 0.0 reduce-scatter.5.cloned.1.call-start
  95.7 2.9 %copy.25 = bf16[2,1,2048,256]{2,3,0,1:T(8,128)(2,1)S(1)} copy(bf16[2,1,2048,256]{3,2,1,0:T(8,128)(2,1)} %param.25) | data formatting | bytes 4194304 | tf_op jit(solution)/shard_map/reshape.28
  98.7 0.4 fusion.45
  99.7 0.1 fusion.44
  99.8 0.1 fusion.53
  99.9 0.2 fusion.23
  100.1 0.1 divide_bitcast_fusion
  100.2 0.1 fusion.32
  100.3 2.6 %reshape.276 = bf16[2048,2,256]{2,1,0:T(2,128)(2,1)S(1)} reshape(bf16[1,2048,512]{2,1,0:T(8,128)(2,1)} %param.26) | data formatting | bytes 4194304 | tf_op jit(solution)/shard_map/reshape.37
  102.9 0.4 fusion
  103.3 0.1 bitcast_add_fusion
  103.4 0.0 copy-done
  103.4 53.5 %reduce-scatter.3.cloned.1.call-done = f32[16,512]{1,0:T(8,128)} async-done(((f32[128,512]{1,0:T(8,128)}), f32[16,512]{1,0:T(8,128)}) %reduce-scatter.3.cloned.1.call-update) | async-done | bytes 32784 | tf_op jit(solution)/shard_map/reduce_scatter | solution.py:124
  156.9 0.8 reshape.277
  157.7 0.1 fusion.19
  157.8 0.1 mul.199
  157.9 3.6 %convolution_convert_fusion = bf16[17,4096]{1,0:T(8,128)(2,1)} fusion(bf16[512,4096]{1,0:T(8,128)(2,1)} %param.20, f32[17,512]{1,0:T(8,128)S(1)} %bitcast.157, f32[1,512]{1,0:T(1,128)S(1)} %bitcast.161, f32[16,512]{1,0:T(8,128)} %reduce-scatter.3.cloned.1.call-done, f32[512]{0:T(512)S(1)} %bitcast.162), kind=kOutput, calls=%fused_computation | convolution fusion | flops 71407616 | bytes 4405248 | tf_op jit(solution)/shard_map/dot_general | solution.py:160
  161.4 0.0 reduce-scatter.5.cloned.1.call-update
  161.5 19.0 %reduce-scatter.5.cloned.1.call-done = bf16[17,1024]{1,0:T(8,128)(2,1)} async-done(((bf16[17,4096]{1,0:T(8,128)(2,1)}), bf16[17,1024]{1,0:T(8,128)(2,1)}) %reduce-scatter.5.cloned.1.call-update) | async-done | bytes 34832 | tf_op jit(solution)/shard_map/reduce_scatter | solution.py:162
  180.5 1.4 slice.242
  181.8 1.3 slice.243
  (33 shorter events, 0.4 us)
Async XLA Ops:
  7.2 96.2 %copy-start = (f32[256]{0:T(256)S(1)}, f32[256]{0:T(256)}, u32[]{:S(2)}) copy-start(f32[256]{0:T(256)} %param.21) | copy-start | bytes 3076
  7.2 36.8 %copy-start.2 = (bf16[16,4096]{1,0:T(8,128)(2,1)S(1)}, bf16[16,4096]{1,0:T(8,128)(2,1)}, u32[]{:S(2)}) copy-start(bf16[16,4096]{1,0:T(8,128)(2,1)} %param.14) | copy-start | bytes 393220
  7.2 36.8 %copy-start.4 = (bf16[1,4096]{1,0:T(2,128)(2,1)S(1)}, bf16[1,4096]{1,0:T(2,128)(2,1)}, u32[]{:S(2)}) copy-start(bf16[1,4096]{1,0:T(2,128)(2,1)} %param.15) | copy-start | bytes 24580
  7.2 36.8 %copy-start.5 = (f32[4096]{0:T(1024)S(1)}, f32[4096]{0:T(1024)}, u32[]{:S(2)}) copy-start(f32[4096]{0:T(1024)} %param.16) | copy-start | bytes 49156
  7.2 149.7 %reduce-scatter.3.cloned.1.call-start = ((), (), s32[]{:S(2)}) async-start(), calls=%async_computation.2 | async-start | bytes 294912 | tf_op jit(solution)/shard_map/reduce_scatter | solution.py:124
  7.3 36.7 %copy-start.1 = (bf16[2,4096,256]{2,1,0:T(8,128)(2,1)S(1)}, bf16[2,4096,256]{2,1,0:T(8,128)(2,1)}, u32[]{:S(2)}) copy-start(bf16[2,4096,256]{2,1,0:T(8,128)(2,1)} %param.18) | copy-start | bytes 12582916
  8.5 36.7 %copy-start.3 = (bf16[2,1024,256]{2,1,0:T(8,128)(2,1)S(1)}, bf16[2,1024,256]{2,1,0:T(8,128)(2,1)}, u32[]{:S(2)}) copy-start(bf16[2,1024,256]{2,1,0:T(8,128)(2,1)} %param.23) | copy-start | bytes 3145732
  45.9 43.4 %copy-start.6 = (f32[2]{0:T(128)S(1)}, f32[2]{0:T(128)}, u32[]{:S(2)}) copy-start(f32[2]{0:T(128)} %param.22) | copy-start | bytes 28
  86.4 7.4 %copy-start.7 = (bf16[1024,512]{1,0:T(8,128)(2,1)S(1)}, bf16[1024,512]{1,0:T(8,128)(2,1)}, u32[]{:S(2)}) copy-start(bf16[1024,512]{1,0:T(8,128)(2,1)} %param.24) | copy-start | bytes 3145732
  95.6 84.9 %reduce-scatter.5.cloned.1.call-start = ((), (), s32[]{:S(2)}) async-start(), calls=%async_computation.3 | async-start | bytes 245760 | tf_op jit(solution)/shard_map/reduce_scatter | solution.py:162
Sparse Core Ops, SparseCore 0:
  95.7 61.1 reduce-scatter.2
  161.6 18.8 reduce-scatter.4
where the time goes:
time: 191 us; the launch traced here: 190 us
  waiting for transfers between devices  72.5 us (38%)
  blocking collectives  70.8 us (37%)
  matrix products  17.9 us (9%)
  between operations  15 us (8%)
  local copies, waits for them, and re-layouts  9.9 us (5%)
  other arithmetic  3.85 us (2%)
    reduce_scatter x1, waiting for transfers between devices, body(): lax.psum_scatter(terms.reshape(total_rows, terms.shape[2]), 'kv', scatter...  53.5 us
    all_gather x1, blocking collectives, body(): gathered = lax.all_gather(query[:piece_rows], 'kv', axis=0, tiled=True)  32.3 us
    pmax x1, blocking collectives, body(): row_top = lax.pmax(local_max, 'kv')  21.4 us
    reduce_scatter x1, waiting for transfers between devices, body(): lax.psum_scatter(partial_value.astype(jnp.bfloat16), 'tp', scatter_dimens...  19 us
    psum x1, blocking collectives, body(): row_sum = lax.psum(local_tot * jnp.exp(local_max - row_top), 'kv')  17.1 us
    another operation x4, local copies, waits for them, and re-layouts  5.52 us
  transfers between devices with their start and end apart: 2, of which 2 were waited for; matrix products, arithmetic and copies ran while one was open for 4% of the time, Pallas kernels for 0%

commit v1 on v0

v1 whole, which is shorter than its diff:
```python
import functools

import jax
import jax.numpy as jnp
from jax import lax
from jax.experimental import pallas as pl
from jax.experimental.pallas import tpu as pltpu
from jax.sharding import PartitionSpec as P

DH = 128
LANES = 128
epsilon = 1e-06
F32 = jnp.float32
BF16 = jnp.bfloat16


def up(n, m):
    return -(-n // m) * m


def dot(a, b):
    return lax.dot_general(a, b, (((1,), (0,)), ((), ())), preferred_element_type=F32)


def dot_t(a, b):
    return lax.dot_general(a, b, (((1,), (1,)), ((), ())), preferred_element_type=F32)


def vmem():
    return pl.BlockSpec(memory_space=pltpu.VMEM)


def smem():
    return pl.BlockSpec(memory_space=pltpu.SMEM)


def hbm():
    return pl.BlockSpec(memory_space=pl.ANY)


def params(mib):
    return pltpu.CompilerParams(vmem_limit_bytes=mib * 1024 * 1024)


def split3(x):
    hi = x.astype(BF16)
    rest = x - hi.astype(F32)
    mid = rest.astype(BF16)
    low = (rest - mid.astype(F32)).astype(BF16)
    return hi.astype(F32), mid.astype(F32), low.astype(F32)


def query_kernel(tok, dec, gain, wq, q_all, q_dec, normed, wbuf, sems, *, copies, steps):
    parts, depth, width = wq.shape
    step = depth // steps
    moves = []
    for c in range(parts):
        for k in range(steps):
            move = pltpu.make_async_copy(
                wq.at[c, pl.ds(k * step, step)], wbuf.at[c, pl.ds(k * step, step)], sems.at[c, k]
            )
            move.start()
            moves.append(move)
    piece_rows = tok.shape[0]
    dec_rows = dec.shape[0]

    def norm(x):
        xf = x.astype(F32)
        mean = jnp.mean(xf * xf, axis=-1, keepdims=True)
        return (xf * lax.rsqrt(mean + epsilon) * gain[...]).astype(BF16)

    normed[...] = jnp.zeros(normed.shape, BF16)
    normed[:piece_rows] = norm(tok[...])
    normed[piece_rows : piece_rows + dec_rows] = norm(dec[...])
    for c in range(parts):
        acc = jnp.zeros((normed.shape[0], width), F32)
        for k in range(steps):
            moves[c * steps + k].wait()
            cut = slice(k * step, (k + 1) * step)
            acc = acc + dot(normed[:, cut], wbuf[c, cut])
        out = acc.astype(BF16)
        cols = slice(c * width, (c + 1) * width)
        for i in range(copies):
            q_all[i, :, cols] = out[:piece_rows]
        q_dec[:, cols] = out[piece_rows:]


def attend_kernel(
    lens, lam, normed, wk, wv, q_all, q_dec, ck, cv, dk, dv, send, dec_att, own_k, own_v,
    *, piece_rows, dec_rows, axis,
):
    scale = DH ** (-0.5)
    width = wk.shape[2]
    heads = width // DH
    total = q_all.shape[0]
    for c in range(2):
        own_k[:, c * width : (c + 1) * width] = dot(normed[...], wk[c]).astype(BF16)
    own_v[...] = dot(normed[...], wv[...]).astype(BF16)

    first = lax.axis_index(axis) * piece_rows
    block = min(128, total)

    def rows(at):
        qpos = at + lax.broadcasted_iota(jnp.int32, (block, piece_rows), 0)
        kpos = first + lax.broadcasted_iota(jnp.int32, (block, piece_rows), 1)
        keep = kpos <= qpos
        lane = lax.broadcasted_iota(jnp.int32, (block, LANES), 1)
        stats = jnp.zeros((block, LANES), F32)
        for h in range(heads):
            vcols = slice(h * 2 * DH, (h + 1) * 2 * DH)
            for c in range(2):
                cols = slice(h * DH, (h + 1) * DH)
                qcols = slice(c * width + h * DH, c * width + (h + 1) * DH)
                q = q_all[pl.ds(at, block), qcols]
                far = dot_t(q, ck[c, :, cols]) * scale
                near = dot_t(q, own_k[:piece_rows, qcols]) * scale
                near = jnp.where(keep, near, -jnp.inf)
                top = jnp.maximum(
                    jnp.max(far, axis=-1, keepdims=True), jnp.max(near, axis=-1, keepdims=True)
                )
                far = jnp.exp(far - top)
                near = jnp.exp(near - top)
                tot = jnp.sum(far, axis=-1, keepdims=True) + jnp.sum(near, axis=-1, keepdims=True)
                out = dot(far.astype(BF16), cv[:, vcols])
                out = out + dot(near.astype(BF16), own_v[:piece_rows, vcols])
                j = 2 * h + c
                base = j * 2 * DH
                send[pl.ds(at, block), base : base + 2 * DH] = out.astype(BF16)
                for g, (a, b) in enumerate(zip(split3(top), split3(tot))):
                    stats = jnp.where(lane == 32 * g + j, a, stats)
                    stats = jnp.where(lane == 32 * g + 2 * heads + j, b, stats)
        base = 4 * width
        send[pl.ds(at, block), base : base + LANES] = stats.astype(BF16)

    if total == block:
        rows(0)
    else:

        def step(i, carry):
            rows(i * block)
            return carry

        lax.fori_loop(0, total // block, step, 0)

    slots = dk.shape[2]
    pad = q_dec.shape[0]
    pos = lax.broadcasted_iota(jnp.int32, (pad, slots), 1)
    row = lax.broadcasted_iota(jnp.int32, (pad, 2 * DH), 0)
    for h in range(heads):
        vcols = slice(h * 2 * DH, (h + 1) * 2 * DH)
        merged = jnp.zeros((pad, 2 * DH), F32)
        for b in range(dec_rows):
            fars, nears = [], []
            for c in range(2):
                cols = slice(h * DH, (h + 1) * DH)
                qcols = slice(c * width + h * DH, c * width + (h + 1) * DH)
                q = q_dec[:, qcols]
                far = dot_t(q, dk[c, b, :, cols]) * scale
                far = jnp.where(pos < lens[b], far, -jnp.inf)
                k = own_k[piece_rows:, qcols].astype(F32)
                near = jnp.sum(q.astype(F32) * k, axis=-1, keepdims=True) * scale
                top = jnp.maximum(jnp.max(far, axis=-1, keepdims=True), near)
                far = jnp.exp(far - top)
                near = jnp.exp(near - top)
                tot = jnp.sum(far, axis=-1, keepdims=True) + near
                fars.append(far / tot)
                nears.append(near / tot)
            far_w = (fars[0] - lam[h] * fars[1]).astype(BF16)
            near_w = (nears[0] - lam[h] * nears[1]).astype(BF16)
            out = dot(far_w, dv[b, :, vcols])
            out = out + near_w.astype(F32) * own_v[piece_rows:, vcols].astype(F32)
            merged = jnp.where(row == b, out, merged)
        dec_att[:, vcols] = merged


def project_kernel(lam, got, dec_att, gain, wo, out, heads_out, *, dec_rows, parts):
    peers, piece_rows, _ = got.shape
    heads = dec_att.shape[1] // (2 * DH)
    base = heads * 4 * DH
    stats = got[:, :, base : base + LANES].astype(F32).reshape(peers * piece_rows, LANES)
    stats = stats + (pltpu.roll(stats, LANES - 32, 1) + pltpu.roll(stats, LANES - 64, 1))
    tots = pltpu.roll(stats, LANES - 2 * heads, 1).reshape(peers, piece_rows, LANES)
    tops = stats.reshape(peers, piece_rows, LANES)
    scale = jnp.exp(tops - jnp.max(tops, axis=0, keepdims=True))
    denom = jnp.sum(scale * tots, axis=0, keepdims=True)
    coef = scale / denom

    def head_norm(att):
        mean = jnp.mean(att * att, axis=-1, keepdims=True)
        return (att * lax.rsqrt(mean + epsilon) * gain[...]).astype(BF16)

    for h in range(heads):
        vcols = slice(h * 2 * DH, (h + 1) * 2 * DH)
        sums = []
        for c in range(2):
            j = 2 * h + c
            acc = jnp.zeros((piece_rows, 2 * DH), F32)
            for s in range(peers):
                part = got[s, :, j * 2 * DH : (j + 1) * 2 * DH].astype(F32)
                acc = acc + coef[s, :, j : j + 1] * part
            sums.append(acc)
        heads_out[:piece_rows, vcols] = head_norm(sums[0] - lam[h] * sums[1])
        heads_out[piece_rows:, vcols] = head_norm(dec_att[:, vcols])
    cols = wo.shape[1] // parts
    chunks = cols // LANES
    for p in range(parts):
        part = dot(heads_out[...], wo[:, p * cols : (p + 1) * cols])
        out[p, :, :cols] = part[:piece_rows].astype(BF16)
        out[p, :, cols:] = jnp.zeros((piece_rows, out.shape[2] - cols), BF16)
        for b in range(dec_rows):
            for k in range(chunks):
                at = b * chunks + k
                lanes = cols + (at // piece_rows) * LANES
                r = at % piece_rows
                row = part[piece_rows + b : piece_rows + b + 1, k * LANES : (k + 1) * LANES]
                out[p, r : r + 1, lanes : lanes + LANES] = row.astype(BF16)


def sum_kernel(*refs, dec_rows):
    *ins, piece, dec = refs
    cols = piece.shape[1]
    piece_rows = piece.shape[0]
    chunks = cols // LANES
    total = ins[0][...].astype(F32)
    for ref in ins[1:]:
        total = total + ref[...].astype(F32)
    out = total.astype(BF16)
    piece[...] = out[:, :cols]
    for b in range(dec_rows):
        for k in range(chunks):
            at = b * chunks + k
            lanes = cols + (at // piece_rows) * LANES
            r = at % piece_rows
            dec[b : b + 1, k * LANES : (k + 1) * LANES] = out[r : r + 1, lanes : lanes + LANES]


def body(
    tokens, dec_tokens, norm_gain, w_query, w_key, w_value, w_out, head_gain, mix_lambda,
    ctx_keys, ctx_values, dec_keys, dec_values, dec_len, *, n_kv, n_tp,
):
    piece_rows, model = tokens.shape
    dec_rows = dec_tokens.shape[0]
    width = w_query.shape[2]
    pad = up(dec_rows, 16)
    rows = piece_rows + pad
    steps = 4
    q_send, q_dec, normed = pl.pallas_call(
        functools.partial(query_kernel, copies=n_kv, steps=steps),
        out_shape=(
            jax.ShapeDtypeStruct((n_kv, piece_rows, 2 * width), BF16),
            jax.ShapeDtypeStruct((pad, 2 * width), BF16),
            jax.ShapeDtypeStruct((rows, model), BF16),
        ),
        in_specs=[vmem(), vmem(), vmem(), hbm()],
        out_specs=(vmem(), vmem(), vmem()),
        scratch_shapes=[
            pltpu.VMEM(w_query.shape, BF16),
            pltpu.SemaphoreType.DMA((2, steps)),
        ],
        compiler_params=params(12),
        name="query_proj",
    )(tokens, dec_tokens, norm_gain.reshape(1, model), w_query)
    q_all = lax.all_to_all(q_send, "kv", 0, 0).reshape(n_kv * piece_rows, 2 * width)
    send, dec_att = pl.pallas_call(
        functools.partial(attend_kernel, piece_rows=piece_rows, dec_rows=dec_rows, axis="kv"),
        out_shape=(
            jax.ShapeDtypeStruct((n_kv * piece_rows, 4 * width + LANES), BF16),
            jax.ShapeDtypeStruct((pad, 2 * width), F32),
        ),
        in_specs=[smem(), smem()] + [vmem()] * 9,
        out_specs=(vmem(), vmem()),
        scratch_shapes=[
            pltpu.VMEM((rows, 2 * width), BF16),
            pltpu.VMEM((rows, 2 * width), BF16),
        ],
        compiler_params=params(40),
        name="attend",
    )(
        dec_len, mix_lambda, normed, w_key, w_value, q_all, q_dec,
        ctx_keys, ctx_values, dec_keys, dec_values,
    )
    got = lax.all_to_all(send.reshape(n_kv, piece_rows, 4 * width + LANES), "kv", 0, 0)
    cols = w_out.shape[1] // n_tp
    extra = up(dec_rows * (cols // LANES), piece_rows) // piece_rows * LANES
    partial = pl.pallas_call(
        functools.partial(project_kernel, dec_rows=dec_rows, parts=n_tp),
        out_shape=jax.ShapeDtypeStruct((n_tp, piece_rows, cols + extra), BF16),
        in_specs=[smem()] + [vmem()] * 4,
        out_specs=vmem(),
        scratch_shapes=[pltpu.VMEM((rows, 2 * width), BF16)],
        compiler_params=params(12),
        name="project",
    )(mix_lambda, got, dec_att, head_gain.reshape(1, 2 * DH), w_out)
    me = lax.axis_index("tp")
    shares = [lax.dynamic_index_in_dim(partial, me, 0, keepdims=False)]
    for s in range(1, n_tp):
        mine = lax.dynamic_index_in_dim(partial, me ^ s, 0, keepdims=False)
        shares.append(lax.ppermute(mine, "tp", [(j, j ^ s) for j in range(n_tp)]))
    return pl.pallas_call(
        functools.partial(sum_kernel, dec_rows=dec_rows),
        out_shape=(
            jax.ShapeDtypeStruct((piece_rows, cols), BF16),
            jax.ShapeDtypeStruct((dec_rows, cols), BF16),
        ),
        in_specs=[vmem()] * n_tp,
        out_specs=(vmem(), vmem()),
        compiler_params=params(4),
        name="final_sum",
    )(*shares)


def solution(mesh):
    in_specs = (
        P("kv", None),
        P("kv", None),
        P(),
        P(None, None, "tp"),
        P(None, None, "tp"),
        P(None, "tp"),
        P("tp", None),
        P(),
        P("tp"),
        P(None, "kv", "tp"),
        P("kv", "tp"),
        P(None, "kv", None, "tp"),
        P("kv", None, "tp"),
        P("kv"),
    )
    out_specs = (P("kv", "tp"), P("kv", "tp"))
    run = functools.partial(body, n_kv=mesh.shape["kv"], n_tp=mesh.shape["tp"])
    return jax.shard_map(run, mesh=mesh, in_specs=in_specs, out_specs=out_specs, check_vma=False)
```

time: 191 us -> 60.2 us (0.32)
  blocking collectives: 70.8 us -> 0 us
  waiting for transfers between devices: 72.5 us -> 18.3 us
  matrix products: 17.9 us -> 0 us
  between operations: 15 us -> 1.38 us
  starting transfers between devices: 0.08 us -> 12.6 us
  Pallas kernels: 0 us -> 10.7 us
  local copies, waits for them, and re-layouts: 9.9 us -> 16.5 us
  other arithmetic: 3.85 us -> 0 us
    reduce_scatter x2 -> x0, waiting for transfers between devices: 72.4 us -> none  [the longest x1 53.5 us: body(): lax.psum_scatter(terms.reshape(total_rows, terms.shape[2]), 'kv', scatter...]
    all_gather x1 -> x0, blocking collectives: 32.3 us -> none  [body(): gathered = lax.all_gather(query[:piece_rows], 'kv', axis=0, tiled=True)]
    pmax x1 -> x0, blocking collectives: 21.4 us -> none  [body(): row_top = lax.pmax(local_max, 'kv')]
    dot_general x18 -> x0, matrix products: 17.9 us -> none  [the longest x1 3.55 us: body(): jnp.dot(heads_out, w_out, preferred_element_type=jnp.float32)]
    psum x1 -> x0, blocking collectives: 17.1 us -> none  [body(): row_sum = lax.psum(local_tot * jnp.exp(local_max - row_top), 'kv')]
    unnamed x21 -> x34, local copies, waits for them, and re-layouts: 0.1 us -> 16.4 us
    all_to_all x0 -> x2, waiting for transfers between devices: none -> 15.1 us  [the longest x1 8.44 us: body(): lax.all_to_all(send.reshape(n_kv, piece_rows, 4 * width + LANES), 'kv', 0...]
    all_to_all x0 -> x2, starting transfers between devices: none -> 10.7 us  [the longest x1 7.31 us: body(): lax.all_to_all(q_send, 'kv', 0, 0).reshape(n_kv * piece_rows, 2 * width)]
  transfers between devices with their start and end apart: 2 -> 5, of which waited for: 2 -> 4; matrix products, arithmetic and copies ran while one was open for 4% -> 0% of each run, Pallas kernels for 0% -> 0%
where the time goes in v1:
time: 60.2 us; the launch traced here: 59.5 us
  waiting for transfers between devices  18.3 us (30%)
  local copies, waits for them, and re-layouts  16.5 us (27%)
  starting transfers between devices  12.6 us (21%)
  Pallas kernels  10.7 us (18%)
  between operations  1.38 us (2%)
    unnamed x34, local copies, waits for them, and re-layouts  16.4 us
    all_to_all x1, waiting for transfers between devices, body(): lax.all_to_all(send.reshape(n_kv, piece_rows, 4 * width + LANES), 'kv', 0...  8.44 us
    all_to_all x1, starting transfers between devices, body(): lax.all_to_all(q_send, 'kv', 0, 0).reshape(n_kv * piece_rows, 2 * width)  7.31 us
    all_to_all x1, waiting for transfers between devices, body(): lax.all_to_all(q_send, 'kv', 0, 0).reshape(n_kv * piece_rows, 2 * width)  6.69 us
    pallas_call x1, Pallas kernels, body(): pl.pallas_call(functools.partial(attend_kernel, piece_rows=piece_rows, de...  6.37 us
    all_to_all x1, starting transfers between devices, body(): lax.all_to_all(send.reshape(n_kv, piece_rows, 4 * width + LANES), 'kv', 0...  3.42 us
    ppermute x3, waiting for transfers between devices, body(): shares.append(lax.ppermute(mine, 'tp', [(j, j ^ s) for j in range(n_tp)]))  3.15 us
    pallas_call x1, Pallas kernels, body(): pl.pallas_call(functools.partial(query_kernel, copies=n_kv, steps=steps),...  1.93 us
  transfers between devices with their start and end apart: 5, of which 4 were waited for; matrix products, arithmetic and copies ran while one was open for 0% of the time, Pallas kernels for 0%

profile of v1, /device:TPU:0, one launch (start us, length us, event | category | flops | bytes accessed | tf_op | source)
XLA Modules:
  0.0 59.5 jit_solution(10376465160279256269)
XLA Ops:
  0.6 0.0 copy-start.1
  0.6 2.2 %copy-done.1 = bf16[2,4096,256]{2,1,0:T(8,128)(2,1)S(1)} copy-done((bf16[2,4096,256]{2,1,0:T(8,128)(2,1)S(1)}, bf16[2,4096,256]{2,1,0:T(8,128)(2,1)}, u32[]{:S(2)}) %copy-start.1) | copy-done | bytes 4194328
  2.8 0.0 copy-start.8
  2.8 0.9 %copy-done.8 = bf16[16,4096]{1,0:T(8,128)(2,1)S(1)} copy-done((bf16[16,4096]{1,0:T(8,128)(2,1)S(1)}, bf16[16,4096]{1,0:T(8,128)(2,1)}, u32[]{:S(2)}) %copy-start.8) | copy-done | bytes 131096
  3.7 0.0 copy-start.12
  3.7 0.7 %copy-done.12 = bf16[1,4096]{1,0:T(2,128)(2,1)S(1)} copy-done((bf16[1,4096]{1,0:T(2,128)(2,1)S(1)}, bf16[1,4096]{1,0:T(2,128)(2,1)}, u32[]{:S(2)}) %copy-start.12) | copy-done | bytes 8216
  4.4 0.0 copy-start.13
  4.4 0.7 %copy-done.13 = f32[4096]{0:T(1024)S(1)} copy-done((f32[4096]{0:T(1024)S(1)}, f32[4096]{0:T(1024)}, u32[]{:S(2)}) %copy-start.13) | copy-done | bytes 16408
  5.2 0.0 copy-start.3
  5.2 0.0 copy-start.5
  5.2 1.9 %query_proj.1 = (bf16[8,16,512]{2,1,0:T(8,128)(2,1)S(1)}, bf16[16,512]{1,0:T(8,128)(2,1)S(1)}, bf16[32,4096]{1,0:T(8,128)(2,1)S(1)}) custom-call(bf16[16,4096]{1,0:T(8,128)(2,1)S(1)} %copy-done.8, bf16[1,4096]{1,0:T(2,128)(2,1)S(1)} %copy-done.12, f32[1,4096]{1,0:T(1,128)S(1)} %bitcast.14, bf16[2,4096,256]{2,1,0:T(8,128)(2,1)S(1)} %copy-done.1), custom_call_target="tpu_custom_call" | custom-call | tf_op jit(solution)/shard_map/query_proj/pallas_call | solution.py:247
  7.1 0.0 copy-start.9
  7.1 0.6 %copy-done.9 = bf16[8,16,512]{2,1,0:T(8,128)(2,1)} copy-done((bf16[8,16,512]{2,1,0:T(8,128)(2,1)}, bf16[8,16,512]{2,1,0:T(8,128)(2,1)S(1)}, u32[]{:S(2)}) %copy-start.9) | copy-done | bytes 131096
  7.8 7.3 %all-to-all-start = ((bf16[8,16,512]{2,1,0:T(8,128)(2,1)}), bf16[8,16,512]{2,1,0:T(8,128)(2,1)S(1)}, u32[]{:S(2)}, u32[]{:S(2)}) async-start(bf16[8,16,512]{2,1,0:T(8,128)(2,1)} %copy-done.9), calls=%async_computation | async-start | bytes 262144 | tf_op jit(solution)/shard_map/all_to_all | solution.py:263
  15.7 6.7 %all-to-all-done = bf16[8,16,512]{2,1,0:T(8,128)(2,1)S(1)} async-done(((bf16[8,16,512]{2,1,0:T(8,128)(2,1)}), bf16[8,16,512]{2,1,0:T(8,128)(2,1)S(1)}, u32[]{:S(2)}, u32[]{:S(2)}) %all-to-all-start) | async-done | bytes 131104 | tf_op jit(solution)/shard_map/all_to_all | solution.py:263
  22.4 0.0 copy-done.3
  22.4 0.0 copy-done.5
  22.4 0.0 copy-start
  22.4 2.2 %copy-done = bf16[2,4096,256]{2,1,0:T(8,128)(2,1)S(1)} copy-done((bf16[2,4096,256]{2,1,0:T(8,128)(2,1)S(1)}, bf16[2,4096,256]{2,1,0:T(8,128)(2,1)}, u32[]{:S(2)}) %copy-start) | copy-done | bytes 4194328
  24.6 0.0 copy-start.4
  24.6 1.6 %copy-done.4 = bf16[1,2048,512]{2,1,0:T(8,128)(2,1)S(1)} copy-done((bf16[1,2048,512]{2,1,0:T(8,128)(2,1)S(1)}, bf16[1,2048,512]{2,1,0:T(8,128)(2,1)}, u32[]{:S(2)}) %copy-start.4) | copy-done | bytes 2097176
  26.2 0.0 copy-start.6
  26.2 1.2 %copy-done.6 = bf16[1024,512]{1,0:T(8,128)(2,1)S(1)} copy-done((bf16[1024,512]{1,0:T(8,128)(2,1)S(1)}, bf16[1024,512]{1,0:T(8,128)(2,1)}, u32[]{:S(2)}) %copy-start.6) | copy-done | bytes 1048600
  27.4 0.0 copy-start.14
  27.4 0.7 %copy-done.14 = f32[2]{0:T(128)S(1)} copy-done((f32[2]{0:T(128)S(1)}, f32[2]{0:T(128)}, u32[]{:S(2)}) %copy-start.14) | copy-done | bytes 32
  28.1 6.4 %attend.1 = (bf16[128,1152]{1,0:T(8,128)(2,1)S(1)}, f32[16,512]{1,0:T(8,128)S(1)}) custom-call(s32[1]{0:T(128)S(6)} %copy.16.lens, f32[2]{0:T(128)S(1)} %copy-done.14, bf16[32,4096]{1,0:T(8,128)(2,1)S(1)} %get-tuple-element.7.normed, bf16[2,4096,256]{2,1,0:T(8,128)(2,1)S(1)} %copy-done, bf16[4096,512]{1,0:T(8,128)(2,1)} %wv.1, ...), custom_call_target="tpu_custom_call" | custom-call | tf_op jit(solution)/shard_map/attend/pallas_call | solution.py:264
  34.5 0.0 copy-start.7
  34.5 0.7 %copy-done.7 = bf16[128,1152]{1,0:T(8,128)(2,1)} copy-done((bf16[128,1152]{1,0:T(8,128)(2,1)}, bf16[128,1152]{1,0:T(8,128)(2,1)S(1)}, u32[]{:S(2)}) %copy-start.7) | copy-done | bytes 294936
  35.2 0.0 copy-start.10
  35.2 0.6 %copy-done.10 = f32[16,512]{1,0:T(8,128)} copy-done((f32[16,512]{1,0:T(8,128)}, f32[16,512]{1,0:T(8,128)S(1)}, u32[]{:S(2)}) %copy-start.10) | copy-done | bytes 32792
  35.8 3.4 %all-to-all-start.1 = ((bf16[8,16,1152]{2,1,0:T(8,128)(2,1)}), bf16[8,16,1152]{2,1,0:T(8,128)(2,1)S(1)}, u32[]{:S(2)}, u32[]{:S(2)}) async-start(bf16[8,16,1152]{2,1,0:T(8,128)(2,1)} %bitcast.13), calls=%async_computation.1 | async-start | bytes 589824 | tf_op jit(solution)/shard_map/all_to_all | solution.py:282
  39.2 8.4 %all-to-all-done.1.got = bf16[8,16,1152]{2,1,0:T(8,128)(2,1)S(1)} async-done(((bf16[8,16,1152]{2,1,0:T(8,128)(2,1)}), bf16[8,16,1152]{2,1,0:T(8,128)(2,1)S(1)}, u32[]{:S(2)}, u32[]{:S(2)}) %all-to-all-start.1) | async-done | bytes 294944 | tf_op jit(solution)/shard_map/all_to_all | solution.py:282
  47.7 0.0 copy-start.2
  47.7 2.2 %copy-done.2 = bf16[512,4096]{1,0:T(8,128)(2,1)S(1)} copy-done((bf16[512,4096]{1,0:T(8,128)(2,1)S(1)}, bf16[512,4096]{1,0:T(8,128)(2,1)}, u32[]{:S(2)}) %copy-start.2) | copy-done | bytes 4194328
  49.9 0.0 copy-start.11
  49.9 0.8 %copy-done.11 = f32[16,512]{1,0:T(8,128)S(1)} copy-done((f32[16,512]{1,0:T(8,128)S(1)}, f32[16,512]{1,0:T(8,128)}, u32[]{:S(2)}) %copy-start.11) | copy-done | bytes 32792
  50.6 0.0 copy-start.15
  50.6 0.7 %copy-done.15 = f32[2]{0:T(128)S(1)} copy-done((f32[2]{0:T(128)S(1)}, f32[2]{0:T(128)}, u32[]{:S(2)}) %copy-start.15) | copy-done | bytes 32
  51.3 0.0 copy-start.16
  51.3 0.7 %copy-done.16 = f32[256]{0:T(256)S(1)} copy-done((f32[256]{0:T(256)S(1)}, f32[256]{0:T(256)}, u32[]{:S(2)}) %copy-start.16) | copy-done | bytes 1048
  52.0 1.7 %project.1 = bf16[4,16,1152]{2,1,0:T(8,128)(2,1)S(1)} custom-call(f32[2]{0:T(128)S(1)} %copy-done.15, bf16[8,16,1152]{2,1,0:T(8,128)(2,1)S(1)} %all-to-all-done.1.got, f32[16,512]{1,0:T(8,128)S(1)} %copy-done.11, f32[1,256]{1,0:T(1,128)S(1)} %bitcast.15, bf16[512,4096]{1,0:T(8,128)(2,1)S(1)} %copy-done.2), custom_call_target="tpu_custom_call" | custom-call | tf_op jit(solution)/shard_map/project/pallas_call | solution.py:285
  53.7 0.1 collective-permute-start
  53.8 1.6 %collective-permute-start.1 = (bf16[16,1152]{1,0:T(8,128)(2,1)S(1)}, bf16[16,1152]{1,0:T(8,128)(2,1)S(1)}, u32[]{:S(2)}, u32[]{:S(2)}) collective-permute-start(bf16[16,1152]{1,0:T(8,128)(2,1)S(1)} %get-tuple-element.13), channel_id=1, source_target_pairs={{0,2},{1,3},{2,0},{3,1},{4,6},{5,7},{6,4},{7,5},{8,10},{9,11},{10,... | collective-permute-start | bytes 110600 | tf_op jit(solution)/shard_map/ppermute | solution.py:298
  55.4 0.3 collective-permute-start.2
  55.7 0.0 collective-permute-done.refs_1_
  55.7 2.2 %collective-permute-done.1.refs_2_ = bf16[16,1152]{1,0:T(8,128)(2,1)S(1)} collective-permute-done((bf16[16,1152]{1,0:T(8,128)(2,1)S(1)}, bf16[16,1152]{1,0:T(8,128)(2,1)S(1)}, u32[]{:S(2)}, u32[]{:S(2)}) %collective-permute-start.1) | collective-permute-done | bytes 36896 | tf_op jit(solution)/shard_map/ppermute | solution.py:298
  57.8 1.0 %collective-permute-done.2.refs_3_ = bf16[16,1152]{1,0:T(8,128)(2,1)S(1)} collective-permute-done((bf16[16,1152]{1,0:T(8,128)(2,1)S(1)}, bf16[16,1152]{1,0:T(8,128)(2,1)S(1)}, u32[]{:S(2)}, u32[]{:S(2)}) %collective-permute-start.2) | collective-permute-done | bytes 36896 | tf_op jit(solution)/shard_map/ppermute | solution.py:298
  58.8 0.6 %final_sum.1 = (bf16[16,1024]{1,0:T(8,128)(2,1)}, bf16[1,1024]{1,0:T(2,128)(2,1)}) custom-call(bf16[16,1152]{1,0:T(8,128)(2,1)S(1)} %get-tuple-element.15.refs_0_, bf16[16,1152]{1,0:T(8,128)(2,1)S(1)} %collective-permute-done.refs_1_, bf16[16,1152]{1,0:T(8,128)(2,1)S(1)} %collective-permute-done.1.refs_2_, bf16[16,1152]{1,0:T(8,128)(2,1)S(1)} %collective-permute-done.2.refs_3_), custom_call_target="tpu_custom_call" | custom-call | tf_op jit(solution)/shard_map/final_sum/pallas_call | solution.py:299
  (1 shorter events, 0.0 us)
Async XLA Ops:
  0.6 2.2 %copy-start.1 = (bf16[2,4096,256]{2,1,0:T(8,128)(2,1)S(1)}, bf16[2,4096,256]{2,1,0:T(8,128)(2,1)}, u32[]{:S(2)}) copy-start(bf16[2,4096,256]{2,1,0:T(8,128)(2,1)} %wq.1) | copy-start | bytes 12582916
  2.8 0.9 %copy-start.8 = (bf16[16,4096]{1,0:T(8,128)(2,1)S(1)}, bf16[16,4096]{1,0:T(8,128)(2,1)}, u32[]{:S(2)}) copy-start(bf16[16,4096]{1,0:T(8,128)(2,1)} %tok.1) | copy-start | bytes 393220
  3.7 0.7 %copy-start.12 = (bf16[1,4096]{1,0:T(2,128)(2,1)S(1)}, bf16[1,4096]{1,0:T(2,128)(2,1)}, u32[]{:S(2)}) copy-start(bf16[1,4096]{1,0:T(2,128)(2,1)} %dec.1) | copy-start | bytes 24580
  4.4 0.7 %copy-start.13 = (f32[4096]{0:T(1024)S(1)}, f32[4096]{0:T(1024)}, u32[]{:S(2)}) copy-start(f32[4096]{0:T(1024)} %param.16) | copy-start | bytes 49156
  5.2 17.2 %copy-start.3 = (bf16[2,1,2048,256]{3,2,1,0:T(8,128)(2,1)S(1)}, bf16[2,1,2048,256]{3,2,1,0:T(8,128)(2,1)}, u32[]{:S(2)}) copy-start(bf16[2,1,2048,256]{3,2,1,0:T(8,128)(2,1)} %dk.1) | copy-start | bytes 6291460
  5.2 17.3 %copy-start.5 = (bf16[2,1024,256]{2,1,0:T(8,128)(2,1)S(1)}, bf16[2,1024,256]{2,1,0:T(8,128)(2,1)}, u32[]{:S(2)}) copy-start(bf16[2,1024,256]{2,1,0:T(8,128)(2,1)} %ck.1) | copy-start | bytes 3145732
  7.1 0.7 %copy-start.9 = (bf16[8,16,512]{2,1,0:T(8,128)(2,1)}, bf16[8,16,512]{2,1,0:T(8,128)(2,1)S(1)}, u32[]{:S(2)}) copy-start(bf16[8,16,512]{2,1,0:T(8,128)(2,1)S(1)} %get-tuple-element.8) | copy-start | bytes 393220
  7.8 14.7 %all-to-all-start = ((bf16[8,16,512]{2,1,0:T(8,128)(2,1)}), bf16[8,16,512]{2,1,0:T(8,128)(2,1)S(1)}, u32[]{:S(2)}, u32[]{:S(2)}) async-start(bf16[8,16,512]{2,1,0:T(8,128)(2,1)} %copy-done.9), calls=%async_computation | async-start | bytes 262144 | tf_op jit(solution)/shard_map/all_to_all | solution.py:263
  22.4 2.2 %copy-start = (bf16[2,4096,256]{2,1,0:T(8,128)(2,1)S(1)}, bf16[2,4096,256]{2,1,0:T(8,128)(2,1)}, u32[]{:S(2)}) copy-start(bf16[2,4096,256]{2,1,0:T(8,128)(2,1)} %wk.1) | copy-start | bytes 12582916
  24.6 1.6 %copy-start.4 = (bf16[1,2048,512]{2,1,0:T(8,128)(2,1)S(1)}, bf16[1,2048,512]{2,1,0:T(8,128)(2,1)}, u32[]{:S(2)}) copy-start(bf16[1,2048,512]{2,1,0:T(8,128)(2,1)} %dv.1) | copy-start | bytes 6291460
  26.2 1.2 %copy-start.6 = (bf16[1024,512]{1,0:T(8,128)(2,1)S(1)}, bf16[1024,512]{1,0:T(8,128)(2,1)}, u32[]{:S(2)}) copy-start(bf16[1024,512]{1,0:T(8,128)(2,1)} %cv.1) | copy-start | bytes 3145732
  27.4 0.7 %copy-start.14 = (f32[2]{0:T(128)S(1)}, f32[2]{0:T(128)}, u32[]{:S(2)}) copy-start(f32[2]{0:T(128)} %lam.3) | copy-start | bytes 28
  34.5 0.7 %copy-start.7 = (bf16[128,1152]{1,0:T(8,128)(2,1)}, bf16[128,1152]{1,0:T(8,128)(2,1)S(1)}, u32[]{:S(2)}) copy-start(bf16[128,1152]{1,0:T(8,128)(2,1)S(1)} %get-tuple-element.10) | copy-start | bytes 884740
  35.2 0.6 %copy-start.10 = (f32[16,512]{1,0:T(8,128)}, f32[16,512]{1,0:T(8,128)S(1)}, u32[]{:S(2)}) copy-start(f32[16,512]{1,0:T(8,128)S(1)} %get-tuple-element.11.dec_att) | copy-start | bytes 98308
  35.8 11.9 %all-to-all-start.1 = ((bf16[8,16,1152]{2,1,0:T(8,128)(2,1)}), bf16[8,16,1152]{2,1,0:T(8,128)(2,1)S(1)}, u32[]{:S(2)}, u32[]{:S(2)}) async-start(bf16[8,16,1152]{2,1,0:T(8,128)(2,1)} %bitcast.13), calls=%async_computation.1 | async-start | bytes 589824 | tf_op jit(solution)/shard_map/all_to_all | solution.py:282
  47.7 2.2 %copy-start.2 = (bf16[512,4096]{1,0:T(8,128)(2,1)S(1)}, bf16[512,4096]{1,0:T(8,128)(2,1)}, u32[]{:S(2)}) copy-start(bf16[512,4096]{1,0:T(8,128)(2,1)} %wo.1) | copy-start | bytes 12582916
  49.9 0.8 %copy-start.11 = (f32[16,512]{1,0:T(8,128)S(1)}, f32[16,512]{1,0:T(8,128)}, u32[]{:S(2)}) copy-start(f32[16,512]{1,0:T(8,128)} %copy-done.10) | copy-start | bytes 98308
  50.6 0.7 %copy-start.15 = (f32[2]{0:T(128)S(1)}, f32[2]{0:T(128)}, u32[]{:S(2)}) copy-start(f32[2]{0:T(128)} %lam.3) | copy-start | bytes 28
  51.3 0.7 %copy-start.16 = (f32[256]{0:T(256)S(1)}, f32[256]{0:T(256)}, u32[]{:S(2)}) copy-start(f32[256]{0:T(256)} %param.21) | copy-start | bytes 3076
  53.7 1.9 %collective-permute-start = (bf16[16,1152]{1,0:T(8,128)(2,1)S(1)}, bf16[16,1152]{1,0:T(8,128)(2,1)S(1)}, u32[]{:S(2)}, u32[]{:S(2)}) collective-permute-start(bf16[16,1152]{1,0:T(8,128)(2,1)S(1)} %get-tuple-element.14), channel_id=1, source_target_pairs={{0,1},{1,0},{2,3},{3,2},{4,5},{5,4},{6,7},{7,6},{8,9},{9,8},{10,11... | collective-permute-start | bytes 110600 | tf_op jit(solution)/shard_map/ppermute | solution.py:298
  53.8 4.0 %collective-permute-start.1 = (bf16[16,1152]{1,0:T(8,128)(2,1)S(1)}, bf16[16,1152]{1,0:T(8,128)(2,1)S(1)}, u32[]{:S(2)}, u32[]{:S(2)}) collective-permute-start(bf16[16,1152]{1,0:T(8,128)(2,1)S(1)} %get-tuple-element.13), channel_id=1, source_target_pairs={{0,2},{1,3},{2,0},{3,1},{4,6},{5,7},{6,4},{7,5},{8,10},{9,11},{10,... | collective-permute-start | bytes 110600 | tf_op jit(solution)/shard_map/ppermute | solution.py:298
  55.4 3.4 %collective-permute-start.2 = (bf16[16,1152]{1,0:T(8,128)(2,1)S(1)}, bf16[16,1152]{1,0:T(8,128)(2,1)S(1)}, u32[]{:S(2)}, u32[]{:S(2)}) collective-permute-start(bf16[16,1152]{1,0:T(8,128)(2,1)S(1)} %get-tuple-element.12), channel_id=1, source_target_pairs={{0,3},{1,2},{2,1},{3,0},{4,7},{5,6},{6,5},{7,4},{8,11},{9,10},{10,... | collective-permute-start | bytes 110600 | tf_op jit(solution)/shard_map/ppermute | solution.py:298
